TPU v7x, 32 devices: a whole 2x2x4 slice. The times are simulated.
32 devices in a mesh: kv: 4 (over y, x), tp: 8 (over z, core).
Axes of the slice: x: 2, y: 2, z: 4, core: 2. Of those that a mesh axis runs over, the one named last changes fastest.
Arguments:
- hidden_in: bfloat16 [16, 4096], P('kv', 'tp'), may hold values from -12 to 12
- mixer_gain: float32 [4096], P('tp'), may hold values from 0.1 to 1.9
- query_weight: bfloat16 [4096, 4096], P('tp', 'kv'), may hold values from -0.09375 to 0.09375
- key_weight: bfloat16 [4096, 4096], P('tp', 'kv'), may hold values from -0.09375 to 0.09375
- value_weight: bfloat16 [4096, 8192], P('tp', 'kv'), may hold values from -0.09375 to 0.09375
- gate_weight: bfloat16 [4096, 8192], P('tp', 'kv'), may hold values from -0.09375 to 0.09375
- decay_rate: float32 [16], P('kv'), may hold values from 0.0005 to 0.15
- prior_state: float32 [16, 16, 256, 512], P('tp', 'kv'), may hold values from -2.5 to 2.5
- key_block: bfloat16 [16, 16, 128, 256], P('tp', 'kv'), may hold values from -1 to 1
- value_block: bfloat16 [16, 16, 128, 512], P('tp', 'kv'), may hold values from -6 to 6
- lengths: int32 [16], P('tp'), may hold values from 1 to 16384, 65536 in all
- group_gain: float32 [8192], P('kv'), may hold values from 0.1 to 1.9
- output_weight: bfloat16 [8192, 4096], P('kv', 'tp'), may hold values from -0.0625 to 0.0625
- channel_gain: float32 [4096], P('tp'), may hold values from 0.1 to 1.9
- hidden_gate: bfloat16 [4096, 11264], P('tp', 'kv'), may hold values from -0.09375 to 0.09375
- hidden_up: bfloat16 [4096, 11264], P('tp', 'kv'), may hold values from -0.09375 to 0.09375
- hidden_down: bfloat16 [11264, 4096], P('kv', 'tp'), may hold values from -0.0546875 to 0.0546875
Outputs:
- layer_out: bfloat16 [16, 4096], P('kv', 'tp')
Inputs may be any that keep to these rules, and one draw needn't show every extreme that they name: Sequence s has lengths[s] earlier positions; slots 0 to (lengths[s] mod 128) - 1 of key_block and value_block hold the turned, scaled keys and the values of its positions from 128 * floor(lengths[s] / 128) on, prior_state holds the state of the positions before them, and the other slots take no part.
All inputs are finite; a program needn't handle non-finite values. No bound on the sum of `lengths` on one device may be relied on, other than what follows from the above.
Results may differ from a plain program's by a relative error of at most 0.029.
Values may be sent and summed in bfloat16 or wider, within the bound.
A program may use at most 64 MiB of HBM per device.

v0:
```python
import jax
import jax.numpy as jnp
from jax import lax
from jax.sharding import PartitionSpec as P

D = 4096


epsilon = 1e-06


def as_sent(value):
    return jax.tree.map(lambda a: a.astype(jnp.bfloat16) if a.dtype == jnp.float32 else a, value)


def rotate(vectors, position):
    half_dim = vectors.shape[-1] // 2
    inverse = 10000.0 ** (-jnp.arange(half_dim, dtype=jnp.float32) / half_dim)
    angles = position.astype(jnp.float32)[:, None, None] * inverse
    cosine_part = jnp.cos(angles)
    sine_part = jnp.sin(angles)
    front_half = vectors[..., :half_dim]
    back_half = vectors[..., half_dim:]
    return jnp.concatenate(
        [
            front_half * cosine_part - back_half * sine_part,
            front_half * sine_part + back_half * cosine_part,
        ],
        axis=-1,
    )


def retain(
    queries,
    keys_new,
    values_new,
    gates,
    decay_rate,
    prior_state,
    key_block,
    value_block,
    lengths,
    group_gain,
):
    batch_rows = queries.shape[0]
    heads_here = decay_rate.shape[0]
    key_width = prior_state.shape[2]
    value_width = prior_state.shape[3]
    block_len = key_block.shape[2]
    rotated = rotate(
        queries.astype(jnp.float32).reshape(batch_rows, heads_here, key_width), lengths
    ).astype(jnp.bfloat16)
    fresh_keys = rotate(
        keys_new.astype(jnp.float32).reshape(batch_rows, heads_here, key_width), lengths
    ) * key_width ** (-0.5)
    fresh_values = values_new.astype(jnp.float32).reshape(batch_rows, heads_here, value_width)
    filled = lengths % block_len
    slots = jnp.arange(block_len, dtype=jnp.int32)
    distance = (filled[:, None] - slots[None, :]).astype(jnp.float32)
    live_slots = (slots[None, :] < filled[:, None])[:, None, :]
    weighting = jnp.where(
        live_slots, jnp.exp(-decay_rate[None, :, None] * distance[:, None, :]), jnp.float32(0.0)
    )
    scores = jnp.einsum("shk,shjk->shj", rotated, key_block, preferred_element_type=jnp.float32)
    block_weights = (scores * weighting).astype(jnp.bfloat16)
    block_term = jnp.einsum(
        "shj,shjv->shv", block_weights, value_block, preferred_element_type=jnp.float32
    )
    rotated_wide = rotated.astype(jnp.float32)
    own_term = jnp.sum(rotated_wide * fresh_keys, axis=-1, keepdims=True) * fresh_values
    carried = jnp.exp(-decay_rate[None, :, None] * (filled[:, None, None] + 1).astype(jnp.float32))
    state_term = carried * jnp.einsum(
        "shk,shkv->shv", rotated_wide, prior_state, precision=lax.Precision.HIGHEST
    )
    retained = own_term + block_term + state_term
    centre = jnp.mean(retained, axis=-1, keepdims=True)
    spread = jnp.mean(jnp.square(retained - centre), axis=-1, keepdims=True)
    normed = (retained - centre) * lax.rsqrt(spread + epsilon)
    gated = (
        jax.nn.silu(gates.astype(jnp.float32)).reshape(batch_rows, heads_here, value_width)
        * normed
        * group_gain.reshape(heads_here, value_width)
    )
    return gated.astype(jnp.bfloat16).reshape(batch_rows, heads_here * value_width)


def local(
    hidden_in,
    mixer_gain,
    query_weight,
    key_weight,
    value_weight,
    gate_weight,
    decay_rate,
    prior_state,
    key_block,
    value_block,
    lengths,
    group_gain,
    output_weight,
    channel_gain,
    hidden_gate,
    hidden_up,
    hidden_down,
):
    local_seqs = lengths.shape[0]
    group_count = lax.axis_size("tp")
    first_row = lax.axis_index("tp") * local_seqs
    stream = hidden_in.astype(jnp.float32)
    scaled_in = (stream * mixer_gain).astype(jnp.bfloat16)
    own_squares = jnp.sum(stream * stream, axis=1)
    own_squares = lax.psum(own_squares, "tp")
    all_rows, all_squares = (
        lax.all_gather(scaled_in, "kv", axis=0, tiled=True),
        lax.all_gather(own_squares.astype(jnp.bfloat16), "kv", axis=0, tiled=True).astype(
            own_squares.dtype
        ),
    )
    weights_in = (query_weight, key_weight, value_weight, gate_weight)
    shaped_rows = all_rows.reshape(group_count, local_seqs, all_rows.shape[1])
    half_seqs = local_seqs // 2
    pieces = []
    for portion in range(2):
        rows_part = shaped_rows[:, portion * half_seqs : (portion + 1) * half_seqs].reshape(
            group_count * half_seqs, all_rows.shape[1]
        )
        terms = tuple(
            (
                jnp.dot(rows_part, matrix, preferred_element_type=jnp.float32)
                for matrix in weights_in
            )
        )
        pieces.append(
            jax.tree.map(
                lambda part: part.astype(jnp.float32),
                lax.psum_scatter(as_sent(terms), "tp", scatter_dimension=0, tiled=True),
            )
        )
    summed = tuple(
        (
            jnp.concatenate([pieces[0][member], pieces[1][member]], axis=0)
            for member in range(len(pieces[0]))
        )
    )
    row_squares = lax.dynamic_slice_in_dim(all_squares, first_row, local_seqs, 0)
    first_scale = lax.rsqrt(row_squares / D + epsilon)[:, None]
    queries = (first_scale * summed[0]).astype(jnp.bfloat16)
    keys_new = (first_scale * summed[1]).astype(jnp.bfloat16)
    values_new = (first_scale * summed[2]).astype(jnp.bfloat16)
    gates = (first_scale * summed[3]).astype(jnp.bfloat16)
    mixed = retain(
        queries,
        keys_new,
        values_new,
        gates,
        decay_rate,
        prior_state,
        key_block,
        value_block,
        lengths,
        group_gain,
    )
    head_terms = jnp.dot(
        lax.all_gather(mixed, "tp", axis=0, tiled=True),
        output_weight,
        preferred_element_type=jnp.float32,
    )
    mixer_out = lax.psum_scatter(
        head_terms.astype(jnp.bfloat16), "kv", scatter_dimension=0, tiled=True
    ).astype(jnp.float32)
    middle = stream + mixer_out
    scaled_mid = (middle * channel_gain).astype(jnp.bfloat16)
    middle_squares = jnp.sum(middle * middle, axis=1)
    middle_squares = lax.psum(middle_squares, "tp")
    middle_rows, middle_all = (
        lax.all_gather(scaled_mid, "kv", axis=0, tiled=True),
        lax.all_gather(middle_squares.astype(jnp.bfloat16), "kv", axis=0, tiled=True).astype(
            middle_squares.dtype
        ),
    )
    channel_terms = (
        jnp.dot(middle_rows, hidden_gate, preferred_element_type=jnp.float32),
        jnp.dot(middle_rows, hidden_up, preferred_element_type=jnp.float32),
    )
    channel_summed = (
        lax.psum_scatter(
            channel_terms[0].astype(jnp.bfloat16), "tp", scatter_dimension=0, tiled=True
        ).astype(jnp.float32),
        lax.psum_scatter(
            channel_terms[1].astype(jnp.bfloat16), "tp", scatter_dimension=0, tiled=True
        ).astype(jnp.float32),
    )
    middle_row_squares = lax.dynamic_slice_in_dim(middle_all, first_row, local_seqs, 0)
    second_scale = lax.rsqrt(middle_row_squares / D + epsilon)[:, None]
    gate_part = second_scale * channel_summed[0]
    up_part = second_scale * channel_summed[1]
    activated = (jax.nn.silu(gate_part) * up_part).astype(jnp.bfloat16)
    unit_terms = jnp.dot(
        lax.all_gather(activated, "tp", axis=0, tiled=True),
        hidden_down,
        preferred_element_type=jnp.float32,
    )
    channel_out = lax.psum_scatter(
        unit_terms.astype(jnp.bfloat16), "kv", scatter_dimension=0, tiled=True
    ).astype(jnp.float32)
    return (middle + channel_out).astype(jnp.bfloat16)


def solution(mesh):
    in_specs = (
        P("kv", "tp"),
        P("tp"),
        P("tp", "kv"),
        P("tp", "kv"),
        P("tp", "kv"),
        P("tp", "kv"),
        P("kv"),
        P("tp", "kv", None, None),
        P("tp", "kv", None, None),
        P("tp", "kv", None, None),
        P("tp"),
        P("kv"),
        P("kv", "tp"),
        P("tp"),
        P("tp", "kv"),
        P("tp", "kv"),
        P("kv", "tp"),
    )
    out_specs = P("kv", "tp")
    return jax.shard_map(local, mesh=mesh, in_specs=in_specs, out_specs=out_specs, check_vma=False)
```

profile of v0, /device:TPU:0, one launch (start us, length us, event | category | flops | bytes accessed | tf_op | source)
XLA Modules:
  0.0 253.7 jit_solution(16599473605607127361)
XLA Ops:
  6.5 0.0 copy-start
  6.5 0.0 all-reduce.19.cloned.1.call-start
  6.5 1.0 fusion.7
  7.5 9.7 %all-gather = bf16[4,4,512]{2,1,0:T(4,128)(2,1)S(1)} all-gather(bf16[1,4,512]{2,1,0:T(4,128)(2,1)S(1)} %get-tuple-element.28), channel_id=1, replica_groups=mesh['kv'=4,'tp'=8] {'kv'}, dimensions={0}, use_global_device_ids=true | all-gather | bytes 20480 | tf_op jit(solution)/shard_map/all_gather | solution.py:114
  17.2 0.0 copy-start.1
  17.3 0.0 copy-start.2
  17.3 2.7 %convolution_convert_fusion.2 = bf16[8,2048]{1,0:T(8,128)(2,1)} fusion(bf16[512,2048]{1,0:T(8,128)(2,1)} %param.21, bf16[8,1,512]{2,0,1:T(8,128)(2,1)S(1)} %copy.26), kind=kOutput, calls=%fused_computation.2 | convolution fusion | flops 16793600 | bytes 2138112 | tf_op jit(solution)/shard_map/dot_general | solution.py:129
  20.0 1.0 convolution_convert_fusion.3
  21.0 1.0 convolution_convert_fusion.4
  22.0 1.0 convolution_convert_fusion.5
  23.0 0.0 copy-start.11
  23.0 0.0 copy-start.7
  23.0 0.9 convolution_convert_fusion.10
  23.9 0.8 convolution_convert_fusion.11
  24.7 0.0 copy-done.4
  24.7 0.9 convolution_convert_fusion.8
  25.6 0.8 convolution_convert_fusion.9
  26.4 0.0 all-reduce.19.cloned.1.call-update
  26.4 0.0 all-reduce.21.cloned.1.call-start
  26.6 0.1 subtract_convert_fusion.1
  26.6 0.1 iota_compare_fusion
  26.7 14.6 %psum.14 = bf16[4]{0:T(256)(128)(2,1)S(1)} all-reduce(f32[4]{0:T(128)S(1)} %get-tuple-element.27), channel_id=1, replica_groups=mesh['kv'=4,'tp'=8] {'tp'}, use_global_device_ids=true, to_apply=%region_1.0 | all-reduce | flops 4 | bytes 24 | tf_op jit(solution)/shard_map/psum | solution.py:112
  41.3 0.0 copy-done.12
  41.3 0.6 dynamic-slice.2
  41.9 0.0 copy-done.9
  41.9 0.7 fusion.35
  43.3 0.2 dynamic-update-slice
  43.5 8.9 %all-reduce = bf16[16]{0:T(256)(128)(2,1)S(1)} all-reduce(bf16[16]{0:T(256)(128)(2,1)S(1)} %dynamic-update-slice), channel_id=1, replica_groups=mesh['kv'=4,'tp'=8] {'kv'}, use_global_device_ids=true, to_apply=%add | all-reduce | flops 16 | bytes 64
  52.5 0.1 multiply_cosine_fusion
  52.6 0.1 multiply_exponential_fusion
  54.0 0.1 add_rsqrt_fusion.2
  54.1 29.0 %all-reduce.19.cloned.1.call-done = (bf16[8,1024]{1,0:T(8,128)(2,1)}, bf16[8,1024]{1,0:T(8,128)(2,1)}, bf16[8,2048]{1,0:T(8,128)(2,1)}, bf16[8,2048]{1,0:T(8,128...) async-done(((bf16[8,1024]{1,0:T(8,128)(2,1)}, bf16[8,1024]{1,0:T(8,128)(2,1)}, ...) | async-done | bytes 196624
  83.0 1.4 dynamic-slice_reduce_fusion.6
  84.5 1.4 dynamic-slice_reduce_fusion.4
  85.9 0.1 fusion.24
  86.0 0.2 fusion.21
  86.3 3.6 %fusion.19 = f32[2,4,1,512]{3,2,1,0:T(1,128)S(1)} fusion(f32[2,4,256,512]{3,2,1,0:T(8,128)} %param.24, bf16[2,4,256,1]{2,1,0,3:T(4,128)(2,1)S(1)} %fusion.30), kind=kOutput, calls=%fused_computation.53 | convolution fusion | flops 12582912 | bytes 4214784 | tf_op jit(solution)/shard_map/shk,shkv->shv/dot_general | solution.py:72
  89.9 1.5 dynamic-slice_reduce_fusion
  91.4 0.1 fusion.10
  91.5 0.1 fusion.29
  91.6 1.5 fusion.27
  93.1 0.2 fusion.32
  93.3 0.2 multiply_reduce_fusion
  93.4 1.5 dynamic-slice_reduce_fusion.2
  94.9 0.1 multiply_convert_fusion
  95.1 14.0 %all-gather.1 = bf16[8,2,2048]{2,1,0:T(2,128)(2,1)S(1)} all-gather(bf16[1,2,2048]{2,1,0:T(2,128)(2,1)S(1)} %reshape.210), channel_id=1, replica_groups=mesh['kv'=4,'tp'=8] {'tp'}, dimensions={0}, use_global_device_ids=true | all-gather | bytes 73728 | tf_op jit(solution)/shard_map/all_gather | solution.py:164
  109.1 2.0 convolution_convert_fusion.7
  111.0 16.0 %all-reduce.10 = bf16[16,512]{1,0:T(8,128)(2,1)S(1)} all-reduce(bf16[16,512]{1,0:T(8,128)(2,1)S(1)} %convolution_convert_fusion.7), channel_id=10, replica_groups=mesh['kv'=4,'tp'=8] {'kv'}, use_global_device_ids=true, to_apply=%region_13.14.clone | all-reduce | flops 8192 | bytes 32768
  127.0 0.0 copy-done.8
  127.0 0.1 multiply_reduce_fusion.1
  127.2 7.2 %all-gather.2 = bf16[4,4,512]{2,1,0:T(4,128)(2,1)S(1)} all-gather(bf16[1,4,512]{2,1,0:T(4,128)(2,1)S(1)} %get-tuple-element.20), channel_id=1, replica_groups=mesh['kv'=4,'tp'=8] {'kv'}, dimensions={0}, use_global_device_ids=true | all-gather | bytes 20480 | tf_op jit(solution)/shard_map/all_gather | solution.py:176
  134.4 13.6 %psum.15 = bf16[4]{0:T(256)(128)(2,1)S(1)} all-reduce(f32[4]{0:T(128)S(1)} %get-tuple-element.19), channel_id=1, replica_groups=mesh['kv'=4,'tp'=8] {'tp'}, use_global_device_ids=true, to_apply=%region_15.16 | all-reduce | flops 4 | bytes 24 | tf_op jit(solution)/shard_map/psum | solution.py:174
  148.0 1.1 convolution_convert_fusion
  149.1 0.2 dynamic-update-slice.1
  149.3 3.0 %convolution_convert_fusion.1 = bf16[16,2816]{1,0:T(8,128)(2,1)} fusion(bf16[16,512]{1,0:T(8,128)(2,1)S(1)} %reshape.213, bf16[512,2816]{1,0:T(8,128)(2,1)} %param.31), kind=kOutput, calls=%fused_computation.1 | convolution fusion | flops 46182400 | bytes 2990080 | tf_op jit(solution)/shard_map/dot_general | solution.py:182
  152.3 8.9 %all-reduce.1 = bf16[16]{0:T(256)(128)(2,1)S(1)} all-reduce(bf16[16]{0:T(256)(128)(2,1)S(1)} %dynamic-update-slice.1), channel_id=1, replica_groups=mesh['kv'=4,'tp'=8] {'kv'}, use_global_device_ids=true, to_apply=%add.1 | all-reduce | flops 16 | bytes 64
  161.2 0.0 all-reduce.21.cloned.1.call-update
  161.2 0.1 add_rsqrt_fusion.1
  161.3 51.1 %all-reduce.21.cloned.1.call-done = (bf16[16,2816]{1,0:T(8,128)(2,1)}, bf16[16,2816]{1,0:T(8,128)(2,1)}) async-done(((bf16[16,2816]{1,0:T(8,128)(2,1)}, bf16[16,2816]{1,0:T(8,128)(2,1)}), (bf16[16,2816]{1,0:T(8,128)(2,1)}, bf16[16,2816]{1,0:T(8,128)(2,1)})) %all-reduce.21.cloned.1.call-update) | async-done | bytes 180240
  212.4 0.9 fusion.6
  213.4 14.6 %all-gather.3 = bf16[8,2,2816]{2,1,0:T(2,128)(2,1)S(1)} all-gather(bf16[1,2,2816]{2,1,0:T(2,128)(2,1)S(1)} %fusion.6), channel_id=1, replica_groups=mesh['kv'=4,'tp'=8] {'tp'}, dimensions={0}, use_global_device_ids=true | all-gather | bytes 101376 | tf_op jit(solution)/shard_map/all_gather | solution.py:199
  227.9 2.3 convolution_convert_fusion.6
  230.2 16.0 %all-reduce.13 = bf16[16,512]{1,0:T(8,128)(2,1)S(1)} all-reduce(bf16[16,512]{1,0:T(8,128)(2,1)S(1)} %convolution_convert_fusion.6), channel_id=13, replica_groups=mesh['kv'=4,'tp'=8] {'kv'}, use_global_device_ids=true, to_apply=%region_18.19.clone | all-reduce | flops 8192 | bytes 32768
  246.2 0.6 add_convert_fusion
  (45 shorter events, 0.4 us)
Async XLA Ops:
  6.5 141.5 %copy-start = (bf16[512,2816]{1,0:T(8,128)(2,1)S(1)}, bf16[512,2816]{1,0:T(8,128)(2,1)}, u32[]{:S(2)}) copy-start(bf16[512,2816]{1,0:T(8,128)(2,1)} %param.32) | copy-start | bytes 8650756
  6.5 76.5 %all-reduce.19.cloned.1.call-start = ((), (), s32[]{:S(2)}) async-start(), calls=%async_computation | async-start | bytes 393216
  17.2 2.8 %copy-start.1 = (bf16[512,2048]{1,0:T(8,128)(2,1)S(1)}, bf16[512,2048]{1,0:T(8,128)(2,1)}, u32[]{:S(2)}) copy-start(bf16[512,2048]{1,0:T(8,128)(2,1)} %param.21) | copy-start | bytes 6291460
  17.3 3.7 %copy-start.2 = (bf16[512,2048]{1,0:T(8,128)(2,1)S(1)}, bf16[512,2048]{1,0:T(8,128)(2,1)}, u32[]{:S(2)}) copy-start(bf16[512,2048]{1,0:T(8,128)(2,1)} %param.22) | copy-start | bytes 6291460
  21.0 2.0 copy-start.3
  22.0 2.7 %copy-start.4 = (bf16[512,1024]{1,0:T(8,128)(2,1)S(1)}, bf16[512,1024]{1,0:T(8,128)(2,1)}, u32[]{:S(2)}) copy-start(bf16[512,1024]{1,0:T(8,128)(2,1)} %param.20) | copy-start | bytes 3145732
  23.0 3.5 %copy-start.10 = (s32[2]{0:T(128)S(1)}, s32[2]{0:T(128)}, u32[]{:S(2)}) copy-start(s32[2]{0:T(128)} %param.27) | copy-start | bytes 28
  23.0 18.3 %copy-start.12 = (u32[32]{0:T(128)S(1)}, u32[32]{0:T(128)}, u32[]{:S(2)}) copy-start(u32[32]{0:T(128)} %constant.69) | copy-start | bytes 388
  23.0 18.9 %copy-start.9 = (u32[32]{0:T(128)S(1)}, u32[32]{0:T(128)}, u32[]{:S(2)}) copy-start(u32[32]{0:T(128)} %constant.57) | copy-start | bytes 388
  23.0 29.5 %copy-start.11 = (f32[4]{0:T(128)S(1)}, f32[4]{0:T(128)}, u32[]{:S(2)}) copy-start(f32[4]{0:T(128)} %param.23) | copy-start | bytes 52
  23.0 29.5 %copy-start.7 = (f32[2048]{0:T(1024)S(1)}, f32[2048]{0:T(1024)}, u32[]{:S(2)}) copy-start(f32[2048]{0:T(1024)} %param.28) | copy-start | bytes 24580
  23.9 62.2 %copy-start.5 = (bf16[2,4,128,256]{3,2,1,0:T(8,128)(2,1)S(1)}, bf16[2,4,128,256]{3,2,1,0:T(8,128)(2,1)}, u32[]{:S(2)}) copy-start(bf16[2,4,128,256]{3,2,1,0:T(8,128)(2,1)} %param.25) | copy-start | bytes 1572868
  26.4 186.0 %all-reduce.21.cloned.1.call-start = ((), (), s32[]{:S(2)}) async-start(), calls=%async_computation.1 | async-start | bytes 360448
  89.9 37.1 %copy-start.6 = (bf16[4,512]{1,0:T(4,128)(2,1)S(1)}, bf16[4,512]{1,0:T(4,128)(2,1)}, u32[]{:S(2)}) copy-start(bf16[4,512]{1,0:T(4,128)(2,1)} %param.17) | copy-start | bytes 12292
  89.9 37.1 %copy-start.8 = (f32[512]{0:T(512)S(1)}, f32[512]{0:T(512)}, u32[]{:S(2)}) copy-start(f32[512]{0:T(512)} %param.30) | copy-start | bytes 6148
Sparse Core Ops, SparseCore 0:
  26.6 56.4 all-reduce.18
  161.3 51.0 all-reduce.20
where the time goes:
time: 255 us; the launch traced here: 254 us
  blocking collectives  123 us (48%)
  waiting for transfers between devices  80.2 us (31%)
  matrix products  22.8 us (9%)
  between operations  15.6 us (6%)
  local copies, waits for them, and re-layouts  7.82 us (3%)
  other arithmetic  3.84 us (2%)
    unnamed x4, waiting for transfers between devices  80.2 us
    unnamed x4, blocking collectives  49.8 us
    psum x1, blocking collectives, local(): own_squares = lax.psum(own_squares, 'tp')  14.6 us
    all_gather x1, blocking collectives, local(): lax.all_gather(activated, 'tp', axis=0, tiled=True)  14.6 us
    all_gather x1, blocking collectives, local(): lax.all_gather(mixed, 'tp', axis=0, tiled=True)  14 us
    psum x1, blocking collectives, local(): middle_squares = lax.psum(middle_squares, 'tp')  13.6 us
    all_gather x1, blocking collectives, local(): lax.all_gather(scaled_in, 'kv', axis=0, tiled=True)  9.66 us
    dot_general x8, matrix products, local(): jnp.dot(rows_part, matrix, preferred_element_type=jnp.float32)  9.1 us
  transfers between devices with their start and end apart: 2, of which 2 were waited for; matrix products, arithmetic and copies ran while one was open for 1% of the time, Pallas kernels for 0%

commit v1 on v0

v1 whole, which is shorter than its diff:
```python
import functools

import jax
import jax.numpy as jnp
from jax import lax
from jax.experimental import pallas as pl
from jax.experimental.pallas import tpu as pltpu
from jax.sharding import PartitionSpec as P

EPS = 1e-06
MESH = pl.DeviceIdType.MESH
F32 = jnp.float32
BF16 = jnp.bfloat16


def up128(n):
    return (n + 127) // 128 * 128


def col_tiles(n, width=512):
    return [(c, min(width, n - c)) for c in range(0, n, width)]


def layer_kernel(
    n_kv, n_tp, H,
    hid, mg, wq, wk, wv, wg, decay, state, kblk, vblk, lens, gg, wo, cg, wgate, wup, wdown, cos, sin,
    out,
    hslots, vq, vk, vv, vg, st, kbv, vbv, vo, vgate, vup, vdown,
    x16, part, sA, rA, sB, rB, qs, ks, vs, gs, ts, mx, mx16, oS, oR, mid, sC, rC, ac, ac16, fS, fR,
    lsem, ssem, rsem,
):
    a = lax.axis_index("kv")
    b = lax.axis_index("tp")
    R, F = hid.shape
    S = lens.shape[0]
    rows = R * n_kv
    DK = state.shape[2]
    DV = state.shape[3]
    BLK = kblk.shape[2]
    FL = wgate.shape[1]
    FP = up128(FL)
    D = F * n_tp
    half = DK // 2

    loads = [
        pltpu.make_async_copy(src, dst, lsem.at[i])
        for i, (src, dst) in enumerate(
            [
                (hid, hslots.at[a]), (wq, vq), (wk, vk), (wv, vv), (wg, vg), (state, st),
                (kblk, kbv), (vblk, vbv), (wo, vo), (wgate, vgate), (wup, vup), (wdown, vdown),
            ]
        )
    ]
    for c in loads:
        c.start()

    barrier = pltpu.get_barrier_semaphore()
    for j in range(1, n_kv):
        pl.semaphore_signal(barrier, inc=1, device_id={"kv": lax.rem(a + j, n_kv)}, device_id_type=MESH)
    for j in range(1, n_tp):
        pl.semaphore_signal(barrier, inc=1, device_id={"tp": lax.rem(b + j, n_tp)}, device_id_type=MESH)
    pl.semaphore_wait(barrier, n_kv + n_tp - 2)

    def gather(buf, axis, me, n, k):
        for j in range(1, n):
            pltpu.make_async_remote_copy(
                src_ref=buf.at[me], dst_ref=buf.at[me], send_sem=ssem.at[k], recv_sem=rsem.at[k],
                device_id={axis: lax.rem(me + j, n)}, device_id_type=MESH,
            ).start()

    def scatter(src, dst, axis, me, n, k):
        for j in range(1, n):
            peer = lax.rem(me + j, n)
            pltpu.make_async_remote_copy(
                src_ref=src.at[peer], dst_ref=dst.at[j - 1], send_sem=ssem.at[k], recv_sem=rsem.at[k],
                device_id={axis: peer}, device_id_type=MESH,
            ).start()

    def share(src, dst, axis, me, n, k):
        for j in range(1, n):
            pltpu.make_async_remote_copy(
                src_ref=src, dst_ref=dst.at[j - 1], send_sem=ssem.at[k], recv_sem=rsem.at[k],
                device_id={axis: lax.rem(me + j, n)}, device_id_type=MESH,
            ).start()

    def wait_for(ref, sem):
        pltpu.make_async_copy(ref, ref, sem).wait()

    def product(x, w, c0):
        for c, width in col_tiles(w.shape[1]):
            part[:, c0 + c : c0 + c + width] = jnp.dot(x, w[:, c : c + width], preferred_element_type=F32)

    def squares(x, c0):
        sq = jnp.broadcast_to(jnp.sum(x * x, axis=1, keepdims=True), (rows, 128))
        high = sq.astype(BF16).astype(F32)
        part[:, c0 : c0 + 128] = high
        part[:, c0 + 128 : c0 + 256] = sq - high

    def stage(dst, width):
        for i in range(n_tp):
            dst[i] = part[i * S : (i + 1) * S, 0:width].astype(BF16)

    def total(sent, got, c, width):
        acc = sent[b, :, c : c + width].astype(F32)
        for j in range(n_tp - 1):
            acc = acc + got[j, :, c : c + width].astype(F32)
        return acc

    def rounded(v):
        return v.astype(BF16).astype(F32)

    loads[0].wait()
    gather(hslots, "kv", a, n_kv, 0)
    wait_for(hslots.at[pl.ds(0, n_kv - 1)], rsem.at[0])
    for i in range(n_kv):
        x16[i * R : (i + 1) * R, :] = hslots[i].astype(F32)
    stream = x16[...]
    scaled_in = (stream * mg[...]).astype(BF16)
    NQ = wq.shape[1]
    NV = wv.shape[1]
    loads[1].wait()
    product(scaled_in, vq, 0)
    loads[2].wait()
    product(scaled_in, vk, NQ)
    squares(stream, 2 * NQ)
    stage(sA, 2 * NQ + 256)
    scatter(sA, rA, "tp", b, n_tp, 1)
    loads[3].wait()
    product(scaled_in, vv, 0)
    loads[4].wait()
    product(scaled_in, vg, NV)
    stage(sB, 2 * NV)
    scatter(sB, rB, "tp", b, n_tp, 2)

    PR = qs.shape[0]
    row = lax.broadcasted_iota(jnp.int32, (PR, 1), 0)
    rate = jnp.zeros((PR, 1), F32)
    filled = jnp.zeros((PR, 1), jnp.int32)
    for h in range(H):
        for s in range(S):
            rate = jnp.where(row == h * S + s, decay[h], rate)
            filled = jnp.where(row == h * S + s, lax.rem(lens[s], BLK), filled)
    slot = lax.broadcasted_iota(jnp.int32, (PR, BLK), 1)
    distance = (filled - slot).astype(F32)
    weighting = jnp.where(slot < filled, jnp.exp(-rate * distance), 0.0)
    carried = jnp.exp(-rate * (filled + 1).astype(F32))
    eye = jnp.where(
        lax.broadcasted_iota(jnp.int32, (DK, DK), 0) == lax.broadcasted_iota(jnp.int32, (DK, DK), 1), 1.0, 0.0
    ).astype(BF16)

    wait_for(rA, rsem.at[1])
    sq = total(sA, rA, 2 * NQ, 128) + total(sA, rA, 2 * NQ + 128, 128)
    scale = lax.rsqrt(sq[:, 0:1] / D + EPS)
    cs = cos[...]
    sn = sin[...]
    for h in range(H):
        for base, dst, factor in ((0, qs, 1.0), (NQ, ks, DK ** (-0.5))):
            front = rounded(scale * total(sA, rA, base + h * DK, half))
            back = rounded(scale * total(sA, rA, base + h * DK + half, half))
            dst[h * S : (h + 1) * S, 0:half] = (front * cs - back * sn) * factor
            dst[h * S : (h + 1) * S, half:DK] = (front * sn + back * cs) * factor
    q8 = qs[...].astype(BF16)
    q8f = q8.astype(F32)
    own = jnp.sum(q8f * ks[...], axis=1, keepdims=True)
    contract_last = (((1,), (1,)), ((), ()))
    loads[6].wait()
    scores = jnp.zeros((PR, BLK), F32)
    for h in range(H):
        for s in range(S):
            one = lax.dot_general(q8, kbv[s, h], contract_last, preferred_element_type=F32)
            scores = jnp.where(row == h * S + s, one, scores)
    block_weights = (scores * weighting).astype(BF16)
    q_columns = lax.dot_general(eye, q8, contract_last, preferred_element_type=F32)
    loads[5].wait()
    for h in range(H):
        for s in range(S):
            i = h * S + s
            column = q_columns[:, i : i + 1]
            for c, width in col_tiles(DV, 128):
                ts[i : i + 1, c : c + width] = jnp.sum(
                    column * st[s, h, :, c : c + width], axis=0, keepdims=True
                )
    loads[7].wait()
    block_term = jnp.zeros((PR, DV), F32)
    for h in range(H):
        for s in range(S):
            one = jnp.dot(block_weights, vbv[s, h], preferred_element_type=F32)
            block_term = jnp.where(row == h * S + s, one, block_term)
    partial = block_term + carried * ts[...]
    wait_for(rB, rsem.at[2])
    for h in range(H):
        vs[h * S : (h + 1) * S, :] = rounded(scale * total(sB, rB, h * DV, DV))
        gs[h * S : (h + 1) * S, :] = rounded(scale * total(sB, rB, NV + h * DV, DV))
    retained = own * vs[...] + partial
    centred = retained - jnp.mean(retained, axis=1, keepdims=True)
    spread = jnp.mean(centred * centred, axis=1, keepdims=True)
    gate = gs[...]
    ts[...] = gate / (1.0 + jnp.exp(-gate)) * (centred * lax.rsqrt(spread + EPS))
    for h in range(H):
        mx[b, :, h * DV : (h + 1) * DV] = (
            ts[h * S : (h + 1) * S, :] * gg[:, h * DV : (h + 1) * DV]
        ).astype(BF16)
    gather(mx, "tp", b, n_tp, 3)
    wait_for(mx.at[pl.ds(0, n_tp - 1)], rsem.at[3])
    for i in range(n_tp):
        mx16[i * S : (i + 1) * S, :] = mx[i].astype(F32)

    loads[8].wait()
    head_terms = jnp.dot(mx16[...].astype(BF16), vo[...], preferred_element_type=F32)
    oS[...] = head_terms.astype(BF16)
    share(oS, oR, "kv", a, n_kv, 4)
    wait_for(oR, rsem.at[4])
    middle = x16[...] + oS[...].astype(F32)
    for j in range(n_kv - 1):
        middle = middle + oR[j].astype(F32)
    x16[...] = middle
    for i in range(n_kv):
        mid[i] = x16[i * R : (i + 1) * R, :]

    scaled_mid = (middle * cg[...]).astype(BF16)
    loads[9].wait()
    product(scaled_mid, vgate, 0)
    loads[10].wait()
    product(scaled_mid, vup, FP)
    squares(middle, 2 * FP)
    stage(sC, 2 * FP + 256)
    scatter(sC, rC, "tp", b, n_tp, 5)
    wait_for(rC, rsem.at[5])
    sq = total(sC, rC, 2 * FP, 128) + total(sC, rC, 2 * FP + 128, 128)
    scale = lax.rsqrt(sq[:, 0:1] / D + EPS)
    for c, width in col_tiles(FL):
        gate = scale * total(sC, rC, c, width)
        up = scale * total(sC, rC, FP + c, width)
        ac[b, :, c : c + width] = (gate / (1.0 + jnp.exp(-gate)) * up).astype(BF16)
    gather(ac, "tp", b, n_tp, 6)
    wait_for(ac.at[pl.ds(0, n_tp - 1)], rsem.at[6])
    for i in range(n_tp):
        ac16[i * S : (i + 1) * S, :] = ac[i].astype(F32)
    loads[11].wait()
    x16[...] = jnp.dot(ac16[...].astype(BF16), vdown[...], preferred_element_type=F32)
    for i in range(n_kv):
        fS[i] = x16[i * R : (i + 1) * R, :].astype(BF16)
    scatter(fS, fR, "kv", a, n_kv, 7)
    wait_for(fR, rsem.at[7])
    result = mid[a] + fS[a].astype(F32)
    for j in range(n_kv - 1):
        result = result + fR[j].astype(F32)
    out[...] = result.astype(BF16)

    for ref, k in (
        (hslots.at[pl.ds(0, n_kv - 1)], 0), (rA, 1), (rB, 2), (mx.at[pl.ds(0, n_tp - 1)], 3), (oR, 4),
        (rC, 5), (ac.at[pl.ds(0, n_tp - 1)], 6), (fR, 7),
    ):
        wait_for(ref, ssem.at[k])


def local(
    n_kv, n_tp,
    hidden_in, mixer_gain, query_weight, key_weight, value_weight, gate_weight, decay_rate, prior_state,
    key_block, value_block, lengths, group_gain, output_weight, channel_gain, hidden_gate, hidden_up, hidden_down,
):
    R, F = hidden_in.shape
    S = lengths.shape[0]
    H = decay_rate.shape[0]
    rows = R * n_kv
    DK, DV = prior_state.shape[2:]
    NQ = query_weight.shape[1]
    NV = value_weight.shape[1]
    FL = hidden_gate.shape[1]
    FP = up128(FL)
    half = DK // 2
    inverse = 10000.0 ** (-jnp.arange(half, dtype=F32) / half)
    angles = lengths.astype(F32)[:, None] * inverse
    pairs = max(8, H * S)
    any_space = pl.BlockSpec(memory_space=pl.ANY)
    vmem = pl.BlockSpec(memory_space=pltpu.VMEM)
    smem = pl.BlockSpec(memory_space=pltpu.SMEM)

    def like(v):
        return pltpu.VMEM(v.shape, v.dtype)

    scratch = [
        pltpu.VMEM((n_kv, R, F), BF16),
        like(query_weight), like(key_weight), like(value_weight), like(gate_weight), like(prior_state),
        like(key_block), like(value_block), like(output_weight), like(hidden_gate), like(hidden_up),
        like(hidden_down),
        pltpu.VMEM((rows, F), F32),
        pltpu.VMEM((rows, max(2 * NQ + 256, 2 * NV, 2 * FP + 256)), F32),
        pltpu.VMEM((n_tp, S, 2 * NQ + 256), BF16),
        pltpu.VMEM((n_tp - 1, S, 2 * NQ + 256), BF16),
        pltpu.VMEM((n_tp, S, 2 * NV), BF16),
        pltpu.VMEM((n_tp - 1, S, 2 * NV), BF16),
        pltpu.VMEM((pairs, DK), F32),
        pltpu.VMEM((pairs, DK), F32),
        pltpu.VMEM((pairs, DV), F32),
        pltpu.VMEM((pairs, DV), F32),
        pltpu.VMEM((pairs, DV), F32),
        pltpu.VMEM((n_tp, S, NV), BF16),
        pltpu.VMEM((rows, NV), F32),
        pltpu.VMEM((rows, F), BF16),
        pltpu.VMEM((n_kv - 1, rows, F), BF16),
        pltpu.VMEM((n_kv, R, F), F32),
        pltpu.VMEM((n_tp, S, 2 * FP + 256), BF16),
        pltpu.VMEM((n_tp - 1, S, 2 * FP + 256), BF16),
        pltpu.VMEM((n_tp, S, FL), BF16),
        pltpu.VMEM((rows, FL), F32),
        pltpu.VMEM((n_kv, R, F), BF16),
        pltpu.VMEM((n_kv - 1, R, F), BF16),
        pltpu.SemaphoreType.DMA((12,)),
        pltpu.SemaphoreType.DMA((8,)),
        pltpu.SemaphoreType.DMA((8,)),
    ]
    return pl.pallas_call(
        functools.partial(layer_kernel, n_kv, n_tp, H),
        out_shape=jax.ShapeDtypeStruct((R, F), BF16),
        in_specs=[
            any_space, vmem, any_space, any_space, any_space, any_space, smem, any_space, any_space, any_space,
            smem, vmem, any_space, vmem, any_space, any_space, any_space, vmem, vmem,
        ],
        out_specs=vmem,
        scratch_shapes=scratch,
        compiler_params=pltpu.CompilerParams(
            collective_id=0, has_side_effects=True, vmem_limit_bytes=60 * 1024 * 1024
        ),
    )(
        hidden_in, mixer_gain[None, :], query_weight, key_weight, value_weight, gate_weight, decay_rate,
        prior_state, key_block, value_block, lengths, group_gain[None, :], output_weight,
        channel_gain[None, :], hidden_gate, hidden_up, hidden_down, jnp.cos(angles), jnp.sin(angles),
    )


def solution(mesh):
    in_specs = (
        P("kv", "tp"), P("tp"), P("tp", "kv"), P("tp", "kv"), P("tp", "kv"), P("tp", "kv"), P("kv"),
        P("tp", "kv", None, None), P("tp", "kv", None, None), P("tp", "kv", None, None), P("tp"), P("kv"),
        P("kv", "tp"), P("tp"), P("tp", "kv"), P("tp", "kv"), P("kv", "tp"),
    )
    body = functools.partial(local, mesh.shape["kv"], mesh.shape["tp"])
    return jax.shard_map(body, mesh=mesh, in_specs=in_specs, out_specs=P("kv", "tp"), check_vma=False)
```

time: 255 us -> 41.4 us (0.16)
  blocking collectives: 123 us -> 0 us
  waiting for transfers between devices: 80.2 us -> 0 us
  Pallas kernels: 0 us -> 38.5 us
  matrix products: 22.8 us -> 0 us
  between operations: 15.6 us -> 0.01 us
  local copies, waits for them, and re-layouts: 7.82 us -> 1.27 us
    unnamed x4 -> x0, waiting for transfers between devices: 80.2 us -> none
    unnamed x4 -> x0, blocking collectives: 49.8 us -> none
    all_gather x4 -> x0, blocking collectives: 45.4 us -> none  [the longest x1 14.6 us: local(): lax.all_gather(activated, 'tp', axis=0, tiled=True)]
    pallas_call x0 -> x1, Pallas kernels: none -> 38.5 us  [local(): pl.pallas_call(functools.partial(layer_kernel, n_kv, n_tp, H), out_shape=...]
    psum x2 -> x0, blocking collectives: 28.2 us -> none  [the longest x1 14.6 us: local(): own_squares = lax.psum(own_squares, 'tp')]
    dot_general x15 -> x0, matrix products: 22.8 us -> none  [the longest x8 9.1 us: local(): jnp.dot(rows_part, matrix, preferred_element_type=jnp.float32)]
    unnamed x42 -> x1, local copies, waits for them, and re-layouts: 7.67 us -> 1.27 us
  transfers between devices with their start and end apart: 2 -> 0, of which waited for: 2 -> 0; matrix products, arithmetic and copies ran while one was open for 1% -> 0% of each run, Pallas kernels for 0% -> 0%
where the time goes in v1:
time: 41.4 us; the launch traced here: 41.2 us
  Pallas kernels  38.5 us (93%)
  other arithmetic  1.35 us (3%)
  local copies, waits for them, and re-layouts  1.27 us (3%)
    pallas_call x1, Pallas kernels, local(): pl.pallas_call(functools.partial(layer_kernel, n_kv, n_tp, H), out_shape=...  38.5 us
    unnamed x1, local copies, waits for them, and re-layouts  1.27 us

profile of v1, /device:TPU:0, one launch (start us, length us, event | category | flops | bytes accessed | tf_op | source)
XLA Modules:
  0.0 41.2 jit_solution(2045880827613091148)
XLA Ops:
  0.0 0.7 %convert_element_type.3 = f32[2]{0:T(128)S(1)} convert(s32[2]{0:T(128)} %lens.1) | non-fusion elementwise | flops 2 | bytes 16 | tf_op jit(solution)/shard_map/convert_element_type | solution.py:273
  0.7 0.7 %multiply_sine_fusion = (f32[2,128]{1,0:T(2,128)}, f32[2,128]{1,0:T(2,128)}) fusion(f32[128]{0:T(128)S(1)} %multiply_power_fusion, f32[2]{0:T(128)S(1)} %convert_element_type.3), kind=kLoop, calls=%fused_computation | loop fusion | flops 256 | bytes 2568 | tf_op jit(solution)/shard_map/sin | solution.py:328
  1.4 38.5 %shard_map.163 = bf16[4,512]{1,0:T(4,128)(2,1)} custom-call(bf16[4,512]{1,0:T(4,128)(2,1)} %hid.1, f32[1,512]{1,0:T(1,128)} %bitcast.4, bf16[512,1024]{1,0:T(8,128)(2,1)} %wq.1, bf16[512,1024]{1,0:T(8,128)(2,1)} %wk.1, bf16[512,2048]{1,0:T(8,128)(2,1)} %wv.1, bf16[512,2048]{1,0:T(8,128)(2,1)} %wg.1, f32[4]{0:T(128)} %decay.1, f32[2,4,256,512]{3,2,1,0:T(8,128)} %state.1, ...), custom_call_target="tpu_custom_call" | custom-call | tf_op jit(solution)/shard_map/pallas_call | solution.py:313
  39.9 1.3 %copy.19 = bf16[4,512]{1,0:T(4,128)(2,1)} copy(bf16[4,512]{1,0:T(4,128)(2,1)} %shard_map.163) | data formatting | bytes 8192
  (1 shorter events, 0.0 us)

commit v2 on v1

--- a/solution.py
+++ b/solution.py
@@ -2,12 +2,14 @@
 
 import jax
 import jax.numpy as jnp
+import numpy as np
 from jax import lax
 from jax.experimental import pallas as pl
 from jax.experimental.pallas import tpu as pltpu
 from jax.sharding import PartitionSpec as P
 
 EPS = 1e-06
+CHUNKS = 2
 MESH = pl.DeviceIdType.MESH
 F32 = jnp.float32
 BF16 = jnp.bfloat16
@@ -21,26 +23,67 @@
     return [(c, min(width, n - c)) for c in range(0, n, width)]
 
 
+def chunks_of(n):
+    width = up128(-(-n // CHUNKS))
+    return [(c, min(width, n - c)) for c in range(0, n, width)]
+
+
+def cos_sin(x):
+    k = jnp.floor(x * (2.0 / np.pi) + 0.5)
+    r = ((x - k * 1.5703125) - k * 4.837512969970703125e-4) - k * 7.54978995489188216e-8
+    z = r * r
+    sn = ((-1.9515295891e-4 * z + 8.3321608736e-3) * z - 1.6666654611e-1) * z * r + r
+    cs = ((2.443315711809948e-5 * z - 1.388731625493765e-3) * z + 4.166664568298827e-2) * z * z - 0.5 * z + 1.0
+    turn = k - 4.0 * jnp.floor(k * 0.25)
+    odd = (turn == 1.0) | (turn == 3.0)
+    cos_sign = jnp.where((turn == 1.0) | (turn == 2.0), -1.0, 1.0)
+    sin_sign = jnp.where(turn >= 2.0, -1.0, 1.0)
+    return cos_sign * jnp.where(odd, sn, cs), sin_sign * jnp.where(odd, cs, sn)
+
+
 def layer_kernel(
     n_kv, n_tp, H,
-    hid, mg, wq, wk, wv, wg, decay, state, kblk, vblk, lens, gg, wo, cg, wgate, wup, wdown, cos, sin,
-    out,
-    hslots, vq, vk, vv, vg, st, kbv, vbv, vo, vgate, vup, vdown,
-    x16, part, sA, rA, sB, rB, qs, ks, vs, gs, ts, mx, mx16, oS, oR, mid, sC, rC, ac, ac16, fS, fR,
-    lsem, ssem, rsem,
+    hid, mg_in, wq, wk, wv, wg, decay_in, state, kblk, vblk, lens_in, gg_in, wo, cg_in, wgate, wup, wdown,
+    inverse_in, out,
+    mg, gg, cg, inverse, decay, lens, hslots, vq, vk, vv, vg, st, kbv, vbv, vo, vgate, vup, vdown,
+    x16, part, sA, rA, sB, rB, sG, rG, qs, ks, vs, gs, ts, mx, mx16, oS, oR, mid, fS, fR,
+    lsem, ssem, rsem, *chunk_refs,
 ):
     a = lax.axis_index("kv")
     b = lax.axis_index("tp")
     R, F = hid.shape
-    S = lens.shape[0]
+    S = lens_in.shape[0]
     rows = R * n_kv
     DK = state.shape[2]
     DV = state.shape[3]
     BLK = kblk.shape[2]
     FL = wgate.shape[1]
-    FP = up128(FL)
     D = F * n_tp
     half = DK // 2
+    pieces = chunks_of(FL)
+    sC, rC, ac, ac16 = (chunk_refs[i :: 4] for i in range(4))
+
+    def peers(axis, me, n):
+        if axis == "kv":
+            return [(lax.rem(me + j, n), j - 1) for j in range(1, n)]
+        chips = n // 2
+        chip, core = me // 2, lax.rem(me, 2)
+        upper = chip // (chips // 2)
+        found = []
+        for i in range(chips - 1):
+            rising = i + (i - chip + chips) // chips
+            down = chips - 1 - i
+            falling = down - (chip - down + chips) // chips
+            other = falling + upper * (rising - falling)
+            for same in (0, 1):
+                found.append(other * 2 + lax.rem(core + same, 2))
+        found.append(chip * 2 + 1 - core)
+        return [(peer, lax.rem(peer - me + n, n) - 1) for peer in found]
+
+    barrier = pltpu.get_barrier_semaphore()
+    for axis, me, n in (("tp", b, n_tp), ("kv", a, n_kv)):
+        for peer, _ in peers(axis, me, n):
+            pl.semaphore_signal(barrier, inc=1, device_id={axis: peer}, device_id_type=MESH)
 
     loads = [
         pltpu.make_async_copy(src, dst, lsem.at[i])
@@ -48,31 +91,25 @@
             [
                 (hid, hslots.at[a]), (wq, vq), (wk, vk), (wv, vv), (wg, vg), (state, st),
                 (kblk, kbv), (vblk, vbv), (wo, vo), (wgate, vgate), (wup, vup), (wdown, vdown),
+                (mg_in, mg), (lens_in, lens), (decay_in, decay), (inverse_in, inverse), (gg_in, gg), (cg_in, cg),
             ]
         )
     ]
-    for c in loads:
-        c.start()
-
-    barrier = pltpu.get_barrier_semaphore()
-    for j in range(1, n_kv):
-        pl.semaphore_signal(barrier, inc=1, device_id={"kv": lax.rem(a + j, n_kv)}, device_id_type=MESH)
-    for j in range(1, n_tp):
-        pl.semaphore_signal(barrier, inc=1, device_id={"tp": lax.rem(b + j, n_tp)}, device_id_type=MESH)
+    for i in (0, 12, 1, 2, 3, 4, 13, 14, 15, 6, 5, 7, 16, 8, 17, 9, 10, 11):
+        loads[i].start()
     pl.semaphore_wait(barrier, n_kv + n_tp - 2)
 
     def gather(buf, axis, me, n, k):
-        for j in range(1, n):
+        for peer, _ in peers(axis, me, n):
             pltpu.make_async_remote_copy(
                 src_ref=buf.at[me], dst_ref=buf.at[me], send_sem=ssem.at[k], recv_sem=rsem.at[k],
-                device_id={axis: lax.rem(me + j, n)}, device_id_type=MESH,
+                device_id={axis: peer}, device_id_type=MESH,
             ).start()
 
     def scatter(src, dst, axis, me, n, k):
-        for j in range(1, n):
-            peer = lax.rem(me + j, n)
+        for peer, slot in peers(axis, me, n):
             pltpu.make_async_remote_copy(
-                src_ref=src.at[peer], dst_ref=dst.at[j - 1], send_sem=ssem.at[k], recv_sem=rsem.at[k],
+                src_ref=src.at[peer], dst_ref=dst.at[slot], send_sem=ssem.at[k], recv_sem=rsem.at[k],
                 device_id={axis: peer}, device_id_type=MESH,
             ).start()
 
@@ -86,9 +123,11 @@
     def wait_for(ref, sem):
         pltpu.make_async_copy(ref, ref, sem).wait()
 
-    def product(x, w, c0):
-        for c, width in col_tiles(w.shape[1]):
-            part[:, c0 + c : c0 + c + width] = jnp.dot(x, w[:, c : c + width], preferred_element_type=F32)
+    def product(x, w, c0, first=0, extent=None):
+        for c, width in col_tiles(w.shape[1] if extent is None else extent):
+            part[:, c0 + c : c0 + c + width] = jnp.dot(
+                x, w[:, first + c : first + c + width], preferred_element_type=F32
+            )
 
     def squares(x, c0):
         sq = jnp.broadcast_to(jnp.sum(x * x, axis=1, keepdims=True), (rows, 128))
@@ -115,6 +154,7 @@
     for i in range(n_kv):
         x16[i * R : (i + 1) * R, :] = hslots[i].astype(F32)
     stream = x16[...]
+    loads[12].wait()
     scaled_in = (stream * mg[...]).astype(BF16)
     NQ = wq.shape[1]
     NV = wv.shape[1]
@@ -127,12 +167,16 @@
     scatter(sA, rA, "tp", b, n_tp, 1)
     loads[3].wait()
     product(scaled_in, vv, 0)
+    stage(sB, NV)
+    scatter(sB, rB, "tp", b, n_tp, 2)
     loads[4].wait()
-    product(scaled_in, vg, NV)
-    stage(sB, 2 * NV)
-    scatter(sB, rB, "tp", b, n_tp, 2)
+    product(scaled_in, vg, 0)
+    stage(sG, NV)
+    scatter(sG, rG, "tp", b, n_tp, 5)
 
     PR = qs.shape[0]
+    for i in (13, 14, 15):
+        loads[i].wait()
     row = lax.broadcasted_iota(jnp.int32, (PR, 1), 0)
     rate = jnp.zeros((PR, 1), F32)
     filled = jnp.zeros((PR, 1), jnp.int32)
@@ -144,6 +188,11 @@
     distance = (filled - slot).astype(F32)
     weighting = jnp.where(slot < filled, jnp.exp(-rate * distance), 0.0)
     carried = jnp.exp(-rate * (filled + 1).astype(F32))
+    seq = lax.broadcasted_iota(jnp.int32, (S, half), 0)
+    position = jnp.zeros((S, half), F32)
+    for s in range(S):
+        position = jnp.where(seq == s, lens[s].astype(F32), position)
+    cs, sn = cos_sin(position * inverse[...])
     eye = jnp.where(
         lax.broadcasted_iota(jnp.int32, (DK, DK), 0) == lax.broadcasted_iota(jnp.int32, (DK, DK), 1), 1.0, 0.0
     ).astype(BF16)
@@ -151,8 +200,6 @@
     wait_for(rA, rsem.at[1])
     sq = total(sA, rA, 2 * NQ, 128) + total(sA, rA, 2 * NQ + 128, 128)
     scale = lax.rsqrt(sq[:, 0:1] / D + EPS)
-    cs = cos[...]
-    sn = sin[...]
     for h in range(H):
         for base, dst, factor in ((0, qs, 1.0), (NQ, ks, DK ** (-0.5))):
             front = rounded(scale * total(sA, rA, base + h * DK, half))
@@ -190,10 +237,13 @@
     wait_for(rB, rsem.at[2])
     for h in range(H):
         vs[h * S : (h + 1) * S, :] = rounded(scale * total(sB, rB, h * DV, DV))
-        gs[h * S : (h + 1) * S, :] = rounded(scale * total(sB, rB, NV + h * DV, DV))
     retained = own * vs[...] + partial
     centred = retained - jnp.mean(retained, axis=1, keepdims=True)
     spread = jnp.mean(centred * centred, axis=1, keepdims=True)
+    loads[16].wait()
+    wait_for(rG, rsem.at[5])
+    for h in range(H):
+        gs[h * S : (h + 1) * S, :] = rounded(scale * total(sG, rG, h * DV, DV))
     gate = gs[...]
     ts[...] = gate / (1.0 + jnp.exp(-gate)) * (centred * lax.rsqrt(spread + EPS))
     for h in range(H):
@@ -217,27 +267,38 @@
     for i in range(n_kv):
         mid[i] = x16[i * R : (i + 1) * R, :]
 
+    loads[17].wait()
     scaled_mid = (middle * cg[...]).astype(BF16)
     loads[9].wait()
-    product(scaled_mid, vgate, 0)
     loads[10].wait()
-    product(scaled_mid, vup, FP)
-    squares(middle, 2 * FP)
-    stage(sC, 2 * FP + 256)
-    scatter(sC, rC, "tp", b, n_tp, 5)
-    wait_for(rC, rsem.at[5])
-    sq = total(sC, rC, 2 * FP, 128) + total(sC, rC, 2 * FP + 128, 128)
-    scale = lax.rsqrt(sq[:, 0:1] / D + EPS)
-    for c, width in col_tiles(FL):
-        gate = scale * total(sC, rC, c, width)
-        up = scale * total(sC, rC, FP + c, width)
-        ac[b, :, c : c + width] = (gate / (1.0 + jnp.exp(-gate)) * up).astype(BF16)
-    gather(ac, "tp", b, n_tp, 6)
-    wait_for(ac.at[pl.ds(0, n_tp - 1)], rsem.at[6])
-    for i in range(n_tp):
-        ac16[i * S : (i + 1) * S, :] = ac[i].astype(F32)
+    for n, (first, extent) in enumerate(pieces):
+        wide = up128(extent)
+        product(scaled_mid, vgate, 0, first, extent)
+        product(scaled_mid, vup, wide, first, extent)
+        if n == 0:
+            squares(middle, 2 * wide)
+        stage(sC[n], sC[n].shape[2])
+        scatter(sC[n], rC[n], "tp", b, n_tp, 8 + 2 * n)
+    for n, (first, extent) in enumerate(pieces):
+        wide = up128(extent)
+        wait_for(rC[n], rsem.at[8 + 2 * n])
+        if n == 0:
+            sq = total(sC[0], rC[0], 2 * wide, 128) + total(sC[0], rC[0], 2 * wide + 128, 128)
+            scale = lax.rsqrt(sq[:, 0:1] / D + EPS)
+        for c, width in col_tiles(extent):
+            gate = scale * total(sC[n], rC[n], c, width)
+            up = scale * total(sC[n], rC[n], wide + c, width)
+            ac[n][b, :, c : c + width] = (gate / (1.0 + jnp.exp(-gate)) * up).astype(BF16)
+        gather(ac[n], "tp", b, n_tp, 9 + 2 * n)
     loads[11].wait()
-    x16[...] = jnp.dot(ac16[...].astype(BF16), vdown[...], preferred_element_type=F32)
+    for n, (first, extent) in enumerate(pieces):
+        wait_for(ac[n].at[pl.ds(0, n_tp - 1)], rsem.at[9 + 2 * n])
+        for i in range(n_tp):
+            ac16[n][i * S : (i + 1) * S, :] = ac[n][i].astype(F32)
+        unit_terms = jnp.dot(
+            ac16[n][...].astype(BF16), vdown[first : first + extent, :], preferred_element_type=F32
+        )
+        x16[...] = unit_terms if n == 0 else x16[...] + unit_terms
     for i in range(n_kv):
         fS[i] = x16[i * R : (i + 1) * R, :].astype(BF16)
     scatter(fS, fR, "kv", a, n_kv, 7)
@@ -245,12 +306,15 @@
     result = mid[a] + fS[a].astype(F32)
     for j in range(n_kv - 1):
         result = result + fR[j].astype(F32)
-    out[...] = result.astype(BF16)
-
-    for ref, k in (
+    out[...] = result
+
+    sent = [
         (hslots.at[pl.ds(0, n_kv - 1)], 0), (rA, 1), (rB, 2), (mx.at[pl.ds(0, n_tp - 1)], 3), (oR, 4),
-        (rC, 5), (ac.at[pl.ds(0, n_tp - 1)], 6), (fR, 7),
-    ):
+        (rG, 5), (fR, 7),
+    ]
+    for n in range(len(pieces)):
+        sent += [(rC[n], 8 + 2 * n), (ac[n].at[pl.ds(0, n_tp - 1)], 9 + 2 * n)]
+    for ref, k in sent:
         wait_for(ref, ssem.at[k])
 
 
@@ -267,29 +331,35 @@
     NQ = query_weight.shape[1]
     NV = value_weight.shape[1]
     FL = hidden_gate.shape[1]
-    FP = up128(FL)
     half = DK // 2
-    inverse = 10000.0 ** (-jnp.arange(half, dtype=F32) / half)
-    angles = lengths.astype(F32)[:, None] * inverse
+    pieces = chunks_of(FL)
+    inverse = jnp.asarray((10000.0 ** (-np.arange(half) / half)).astype(np.float32)[None, :])
     pairs = max(8, H * S)
     any_space = pl.BlockSpec(memory_space=pl.ANY)
     vmem = pl.BlockSpec(memory_space=pltpu.VMEM)
-    smem = pl.BlockSpec(memory_space=pltpu.SMEM)
 
     def like(v):
         return pltpu.VMEM(v.shape, v.dtype)
 
     scratch = [
+        pltpu.VMEM((1, F), F32),
+        pltpu.VMEM((1, NV), F32),
+        pltpu.VMEM((1, F), F32),
+        pltpu.VMEM((1, half), F32),
+        pltpu.SMEM((H,), F32),
+        pltpu.SMEM((S,), jnp.int32),
         pltpu.VMEM((n_kv, R, F), BF16),
         like(query_weight), like(key_weight), like(value_weight), like(gate_weight), like(prior_state),
         like(key_block), like(value_block), like(output_weight), like(hidden_gate), like(hidden_up),
         like(hidden_down),
         pltpu.VMEM((rows, F), F32),
-        pltpu.VMEM((rows, max(2 * NQ + 256, 2 * NV, 2 * FP + 256)), F32),
+        pltpu.VMEM((rows, max(2 * NQ + 256, 2 * NV, 2 * up128(pieces[0][1]) + 256)), F32),
         pltpu.VMEM((n_tp, S, 2 * NQ + 256), BF16),
         pltpu.VMEM((n_tp - 1, S, 2 * NQ + 256), BF16),
-        pltpu.VMEM((n_tp, S, 2 * NV), BF16),
-        pltpu.VMEM((n_tp - 1, S, 2 * NV), BF16),
+        pltpu.VMEM((n_tp, S, NV), BF16),
+        pltpu.VMEM((n_tp - 1, S, NV), BF16),
+        pltpu.VMEM((n_tp, S, NV), BF16),
+        pltpu.VMEM((n_tp - 1, S, NV), BF16),
         pltpu.VMEM((pairs, DK), F32),
         pltpu.VMEM((pairs, DK), F32),
         pltpu.VMEM((pairs, DV), F32),
@@ -300,23 +370,24 @@
         pltpu.VMEM((rows, F), BF16),
         pltpu.VMEM((n_kv - 1, rows, F), BF16),
         pltpu.VMEM((n_kv, R, F), F32),
-        pltpu.VMEM((n_tp, S, 2 * FP + 256), BF16),
-        pltpu.VMEM((n_tp - 1, S, 2 * FP + 256), BF16),
-        pltpu.VMEM((n_tp, S, FL), BF16),
-        pltpu.VMEM((rows, FL), F32),
         pltpu.VMEM((n_kv, R, F), BF16),
         pltpu.VMEM((n_kv - 1, R, F), BF16),
-        pltpu.SemaphoreType.DMA((12,)),
-        pltpu.SemaphoreType.DMA((8,)),
-        pltpu.SemaphoreType.DMA((8,)),
+        pltpu.SemaphoreType.DMA((18,)),
+        pltpu.SemaphoreType.DMA((8 + 2 * len(pieces),)),
+        pltpu.SemaphoreType.DMA((8 + 2 * len(pieces),)),
     ]
+    for n, (_, extent) in enumerate(pieces):
+        columns = 2 * up128(extent) + (256 if n == 0 else 0)
+        scratch += [
+            pltpu.VMEM((n_tp, S, columns), BF16),
+            pltpu.VMEM((n_tp - 1, S, columns), BF16),
+            pltpu.VMEM((n_tp, S, extent), BF16),
+            pltpu.VMEM((rows, extent), F32),
+        ]
     return pl.pallas_call(
         functools.partial(layer_kernel, n_kv, n_tp, H),
-        out_shape=jax.ShapeDtypeStruct((R, F), BF16),
-        in_specs=[
-            any_space, vmem, any_space, any_space, any_space, any_space, smem, any_space, any_space, any_space,
-            smem, vmem, any_space, vmem, any_space, any_space, any_space, vmem, vmem,
-        ],
+        out_shape=jax.ShapeDtypeStruct((R, F), F32),
+        in_specs=[any_space] * 18,
         out_specs=vmem,
         scratch_shapes=scratch,
         compiler_params=pltpu.CompilerParams(
@@ -325,8 +396,8 @@
     )(
         hidden_in, mixer_gain[None, :], query_weight, key_weight, value_weight, gate_weight, decay_rate,
         prior_state, key_block, value_block, lengths, group_gain[None, :], output_weight,
-        channel_gain[None, :], hidden_gate, hidden_up, hidden_down, jnp.cos(angles), jnp.sin(angles),
-    )
+        channel_gain[None, :], hidden_gate, hidden_up, hidden_down, inverse,
+    ).astype(BF16)
 
 
 def solution(mesh):

time: 41.4 us -> 37.3 us (0.901)
  Pallas kernels: 38.5 us -> 35.8 us
  local copies, waits for them, and re-layouts: 1.27 us -> 0 us
    pallas_call x1, Pallas kernels: 38.5 us -> 35.8 us  [local(): pl.pallas_call(functools.partial(layer_kernel, n_kv, n_tp, H), out_shape=...]
    unnamed x1 -> x0, local copies, waits for them, and re-layouts: 1.27 us -> none
    sin x1 -> x0, other arithmetic: 0.68 us -> none  [local(): jnp.sin(angles)]
    convert_element_type x1, other arithmetic: 0.66 us -> 1.29 us  [local(): return pl.pallas_call(functools.partial(layer_kernel, n_kv, n_tp, H), out...]
where the time goes in v2:
time: 37.3 us; the launch traced here: 37.1 us
  Pallas kernels  35.8 us (96%)
  other arithmetic  1.29 us (3%)
    pallas_call x1, Pallas kernels, local(): pl.pallas_call(functools.partial(layer_kernel, n_kv, n_tp, H), out_shape=...  35.8 us
    convert_element_type x1, other arithmetic, local(): return pl.pallas_call(functools.partial(layer_kernel, n_kv, n_tp, H), out...  1.29 us

profile of v2, /device:TPU:0, one launch (start us, length us, event | category | flops | bytes accessed | tf_op | source)
XLA Modules:
  0.0 37.1 jit_solution(2084655975677014769)
XLA Ops:
  0.0 35.8 %shard_map.172 = f32[4,512]{1,0:T(4,128)} custom-call(bf16[4,512]{1,0:T(4,128)(2,1)} %hid.1, f32[1,512]{1,0:T(1,128)} %bitcast.4, bf16[512,1024]{1,0:T(8,128)(2,1)} %wq.1, bf16[512,1024]{1,0:T(8,128)(2,1)} %wk.1, bf16[512,2048]{1,0:T(8,128)(2,1)} %wv.1, bf16[512,2048]{1,0:T(8,128)(2,1)} %wg.1, f32[4]{0:T(128)} %decay_in.1, f32[2,4,256,512]{3,2,1,0:T(8,128)} %state.1, ...), custom_call_target="tpu_custom_call" | custom-call | tf_op jit(solution)/shard_map/pallas_call | solution.py:387
  35.8 1.3 %convert_element_type.3 = bf16[4,512]{1,0:T(4,128)(2,1)} convert(f32[4,512]{1,0:T(4,128)} %shard_map.172) | non-fusion elementwise | flops 2048 | bytes 12288 | tf_op jit(solution)/shard_map/convert_element_type | solution.py:400
